TPU v7x, 32 devices: a whole 2x2x4 slice. The times are simulated.
32 devices in a mesh: ep: 8 (over z, y), tp: 4 (over x, core).
Axes of the slice: x: 2, y: 2, z: 4, core: 2. Of those that a mesh axis runs over, the one named last changes fastest.
Arguments:
- tokens: bfloat16 [2048, 2048], P('ep'), may hold values from -6 to 6
- expert_ids: int32 [2048, 2], P('ep'), may hold values from 0 to 7, all different within a row; in each aligned block of 256 rows (0 to 255, 256 to 511, ...) at most 192 rows name the same one
- route_weight: float32 [2048, 2], P('ep'), may hold values from 0.1 to 1
- norm_gain: float32 [2048], replicated, may hold values from 0.1 to 1.9
- expert_gate: bfloat16 [8, 2048, 2048], P('ep', None, 'tp'), may hold values from -4 to 4
- expert_up: bfloat16 [8, 2048, 2048], P('ep', None, 'tp'), may hold values from -4 to 4
- expert_down: bfloat16 [8, 2048, 2048], P('ep', 'tp'), may hold values from -0.03125 to 0.03125
Outputs:
- combined: bfloat16 [2048, 2048], P('ep', 'tp')
Inputs may be any that keep to these rules, and one draw needn't show every extreme that they name: `expert_ids`: each row names 2 different experts. In each aligned block of 256 rows (the rows of one index of ep) no expert is named by more than 192 rows, and in some block one expert is named by exactly 192 rows.
All inputs are finite; a program needn't handle non-finite values.
Results may differ from a plain program's by a relative error of at most 0.012.
Values may be sent and summed in bfloat16 or wider, within the bound.
A program may use at most 128 MiB of HBM per device.

v0:
```python
import jax
import jax.numpy as jnp
from jax import lax
from jax.sharding import PartitionSpec as P

NORM_EPS = 1e-06
CLAMP_LIMIT = 7.0
SWISH_SCALE = 1.702


def normalize(tokens, norm_gain):
    values = tokens.astype(jnp.float32)
    scaled = values * lax.rsqrt(jnp.mean(values * values, axis=-1, keepdims=True) + NORM_EPS)
    return (scaled * norm_gain).astype(jnp.bfloat16)


def activate(gate_sum, up_sum):
    gate_cut = jnp.minimum(gate_sum, CLAMP_LIMIT)
    up_cut = jnp.clip(up_sum, -CLAMP_LIMIT, CLAMP_LIMIT)
    return ((up_cut + 1.0) * gate_cut * jax.nn.sigmoid(SWISH_SCALE * gate_cut)).astype(jnp.bfloat16)


def shards(tokens, expert_ids, route_weight, norm_gain, expert_gate, expert_up, expert_down):
    groups = lax.axis_size("ep")
    tp_count = lax.axis_size("tp")
    member_count = expert_gate.shape[0]
    experts = groups * member_count
    tok_count, model_width = tokens.shape
    top_count = expert_ids.shape[1]
    capacity = min(tok_count, 3 * tok_count * top_count // experts)
    quarter = model_width // tp_count
    normed = normalize(tokens, norm_gain)
    flat_ids = expert_ids.reshape(-1)
    onehot = (flat_ids[:, None] == jnp.arange(experts, dtype=jnp.int32)[None, :]).astype(jnp.int32)
    slot_index = jnp.sum(jnp.cumsum(onehot, axis=0) * onehot, axis=1) - 1
    position = flat_ids * capacity + slot_index
    token_index = jnp.arange(flat_ids.shape[0], dtype=jnp.int32) // top_count
    row_table = jnp.full((experts * capacity,), tok_count, jnp.int32).at[position].set(token_index)
    padded = jnp.concatenate([normed, jnp.zeros((1, model_width), jnp.bfloat16)], axis=0)
    offset = lax.axis_index("tp") * quarter
    source_rows = lax.dynamic_slice_in_dim(padded, offset, quarter, 1)
    send_rows = source_rows[row_table].reshape(groups, member_count, capacity, quarter)
    received = lax.all_to_all(send_rows, "ep", split_axis=0, concat_axis=0, tiled=True)
    slot_count = received.shape[2]
    shard_piece = lax.all_gather(received, "tp", axis=3, tiled=True)
    span_size = shard_piece.shape[3]
    member = 0
    row_block = shard_piece[:, member].reshape(-1, span_size)
    gate_rows = expert_gate[member]
    up_rows = expert_up[member]
    gate_list = [jnp.dot(row_block, gate_rows, preferred_element_type=jnp.float32)]
    up_list = [jnp.dot(row_block, up_rows, preferred_element_type=jnp.float32)]
    gate_sum = jnp.stack(gate_list)
    up_sum = jnp.stack(up_list)
    activated = activate(gate_sum, up_sum)
    member = 0
    weight_rows = expert_down[member]
    product = lax.dot_general(
        weight_rows, activated[member], (((0,), (1,)), ((), ())), preferred_element_type=jnp.float32
    )
    term_list = [product.reshape(quarter * lax.axis_size("tp"), groups, slot_count)]
    summed = lax.psum_scatter(
        jnp.stack(term_list, axis=2).astype(jnp.bfloat16), "tp", scatter_dimension=0, tiled=True
    )
    returned = lax.all_to_all(
        summed.reshape(quarter, experts * capacity), "ep", split_axis=1, concat_axis=1, tiled=True
    )
    picked = jnp.take(returned, position, axis=1).reshape(quarter, tok_count, top_count)
    weighted = jnp.sum(picked.astype(jnp.float32) * route_weight[None, :, :], axis=2)
    return weighted.T.astype(jnp.bfloat16)


def solution(mesh):
    return jax.shard_map(
        shards,
        mesh=mesh,
        in_specs=(
            P("ep", None),
            P("ep", None),
            P("ep", None),
            P(),
            P("ep", None, "tp"),
            P("ep", None, "tp"),
            P("ep", "tp", None),
        ),
        out_specs=P("ep", "tp"),
        check_vma=False,
    )
```

profile of v0, /device:TPU:0, one launch (start us, length us, event | category | flops | bytes accessed | tf_op | source)
XLA Modules:
  0.0 245.8 jit_solution(14064720156240668413)
XLA Ops:
  6.5 0.0 copy-start
  6.5 0.0 all-gather.2.cloned.1.call-start
  6.5 1.0 copy.19
  7.5 0.1 eq.26
  7.7 0.1 reshape.111
  7.8 0.7 broadcast_multiply_fusion
  8.5 1.1 reduce-window.6
  9.6 0.2 slice_reduce_fusion
  9.9 0.1 fusion.12
  10.0 0.1 copy.23
  10.1 0.1 mul.76
  10.3 2.5 scatter_custom_fusion
  12.8 1.5 fusion.4
  14.3 1.5 fusion.6
  15.9 5.4 %gather_fusion = bf16[1536,512]{1,0:T(8,128)(2,1)} fusion(bf16[257,512]{1,0:T(8,128)(2,1)S(1)} %pad_dynamic-slice_fusion, s32[2048]{0:T(1024)S(1)} %pad_clamp_fusion), kind=kCustom, calls=%fused_computation | custom fusion | bytes 3151872 | tf_op jit(solution)/shard_map/gather | solution.py:42
  21.3 44.4 %all_to_all.17 = bf16[8,1,192,512]{3,2,1,0:T(8,128)(2,1)} all-to-all(bf16[8,1,192,512]{3,2,1,0:T(8,128)(2,1)} %bitcast.37), channel_id=1, replica_groups=mesh['ep'=8,'tp'=4] {'ep'}, dimensions={0} | all-to-all | bytes 3145728 | tf_op jit(solution)/shard_map/all_to_all | solution.py:43
  65.7 0.0 all-gather.2.cloned.1.call-update
  65.8 0.0 reduce-scatter.2.cloned.1.call-start
  65.8 45.5 %all-gather.2.cloned.1.call-done = bf16[8,1,192,2048]{3,2,1,0:T(8,128)(2,1)} async-done(((bf16[8,1,192,512]{3,2,1,0:T(8,128)(2,1)}), bf16[8,1,192,2048]{3,2,1,0:T(8,128)(2,1)}) %all-gather.2.cloned.1.call-update) | async-done | bytes 6291472 | tf_op jit(solution)/shard_map/all_gather | solution.py:45
  111.3 8.5 %convolution_minimum_fusion = f32[1536,512]{1,0:T(8,128)} fusion(bf16[1536,2048]{1,0:T(8,128)(2,1)} %bitcast.43, bf16[1,2048,512]{2,1,0:T(8,128)(2,1)} %param.11), kind=kOutput, calls=%fused_computation.5 | convolution fusion | flops 3222011904 | bytes 11534336 | tf_op jit(solution)/shard_map/dot_general | solution.py:51
  119.8 0.0 copy-done
  119.8 11.9 %convolution_convert_fusion = bf16[1536,2048]{1,0:T(8,128)(2,1)} fusion(bf16[1,512,2048]{2,1,0:T(8,128)(2,1)S(1)} %copy-done, f32[1536,512]{1,0:T(8,128)} %convolution_minimum_fusion, bf16[1536,2048]{1,0:T(8,128)(2,1)} %bitcast.44, bf16[1,2048,512]{2,1,0:T(8,128)(2,1)} %param.12), kind=kOutput, calls=%fused_computation.3 | convolution fusion | flops 6452674560 | bytes 19922944 | tf_op jit(solution)/shard_map/dot_general | solution.py:58
  131.7 0.0 reduce-scatter.2.cloned.1.call-update
  131.7 0.0 copy-start.1
  131.7 0.0 copy-start.2
  131.7 58.0 %reduce-scatter.2.cloned.1.call-done = bf16[512,8,1,192]{0,3,1,2:T(8,128)(2,1)} async-done(((bf16[2048,8,1,192]{0,3,1,2:T(8,128)(2,1)}), bf16[512,8,1,192]{0,3,1,2:T(8,128)(2,1)}) %reduce-scatter.2.cloned.1.call-update) | async-done | bytes 1572880 | tf_op jit(solution)/shard_map/reduce_scatter | solution.py:62
  189.7 5.5 %all-to-all-start.1 = ((bf16[512,8,192]{0,2,1:T(8,128)(2,1)}), bf16[512,8,192]{0,2,1:T(8,128)(2,1)}, u32[]{:S(2)}, u32[]{:S(2)}) async-start(bf16[512,8,192]{0,2,1:T(8,128)(2,1)} %bitcast.39), calls=%async_computation.2 | async-start | bytes 3145728 | tf_op jit(solution)/shard_map/all_to_all | solution.py:65
  195.2 0.1 sub.15
  195.4 0.1 copy.21
  195.5 0.0 copy-done.1
  195.5 0.2 copy.22
  195.7 0.0 copy-done.2
  195.7 0.1 copy.25
  195.8 36.3 %all-to-all-done.1 = bf16[512,8,192]{0,2,1:T(8,128)(2,1)} async-done(((bf16[512,8,192]{0,2,1:T(8,128)(2,1)}), bf16[512,8,192]{0,2,1:T(8,128)(2,1)}, u32[]{:S(2)}, u32[]{:S(2)}) %all-to-all-start.1) | async-done | bytes 1572896 | tf_op jit(solution)/shard_map/all_to_all | solution.py:65
  232.2 3.6 %gather_fusion.1 = bf16[512,512]{1,0:T(8,128)(2,1)S(1)} fusion(bf16[512,1536]{0,1:T(8,128)(2,1)} %bitcast.13, s32[1024]{0:T(1024)S(1)} %pad_clamp_fusion.1), kind=kCustom, calls=%fused_computation.1 | custom fusion | bytes 1050624 | tf_op jit(solution)/shard_map/jit(_take)/gather | solution.py:68
  235.8 0.2 gather.11
  236.0 2.9 %multiply_reduce_fusion = bf16[512,256]{0,1:T(8,128)(2,1)} fusion(bf16[512,256,2]{0,2,1:T(2,128)(2,1)S(1)} %gather.11, pred[256,2]{1,0:T(8,128)(4,1)S(1)} %copy.22, f32[256,2]{1,0:T(8,128)S(1)} %copy.25), kind=kLoop, calls=%fused_computation.19 | loop fusion | flops 917504 | bytes 788992 | tf_op jit(solution)/shard_map/reduce_sum | solution.py:69
  (12 shorter events, 0.1 us)
Async XLA Ops:
  6.5 113.3 %copy-start = (bf16[1,512,2048]{2,1,0:T(8,128)(2,1)S(1)}, bf16[1,512,2048]{2,1,0:T(8,128)(2,1)}, u32[]{:S(2)}) copy-start(bf16[1,512,2048]{2,1,0:T(8,128)(2,1)} %param.13) | copy-start | bytes 6291460
  6.5 104.7 %all-gather.2.cloned.1.call-start = ((), (), s32[]{:S(2)}) async-start(), calls=%async_computation.3 | async-start | bytes 7864320 | tf_op jit(solution)/shard_map/all_gather | solution.py:45
  65.8 124.0 %reduce-scatter.2.cloned.1.call-start = ((), (), s32[]{:S(2)}) async-start(), calls=%async_computation.4 | async-start | bytes 7864320 | tf_op jit(solution)/shard_map/reduce_scatter | solution.py:62
  131.7 63.8 %copy-start.1 = (s32[256,2]{0,1:T(2,128)S(1)}, s32[256,2]{0,1:T(2,128)}, u32[]{:S(2)}) copy-start(s32[256,2]{0,1:T(2,128)} %param.8) | copy-start | bytes 6148
  131.7 64.0 %copy-start.2 = (f32[256,2]{0,1:T(2,128)S(1)}, f32[256,2]{0,1:T(2,128)}, u32[]{:S(2)}) copy-start(f32[256,2]{0,1:T(2,128)} %param.9) | copy-start | bytes 6148
  189.7 42.4 %all-to-all-start.1 = ((bf16[512,8,192]{0,2,1:T(8,128)(2,1)}), bf16[512,8,192]{0,2,1:T(8,128)(2,1)}, u32[]{:S(2)}, u32[]{:S(2)}) async-start(bf16[512,8,192]{0,2,1:T(8,128)(2,1)} %bitcast.39), calls=%async_computation.2 | async-start | bytes 3145728 | tf_op jit(solution)/shard_map/all_to_all | solution.py:65
Sparse Core Ops, SparseCore 0:
  65.9 45.3 all-gather.1
  131.8 57.8 reduce-scatter.1
where the time goes:
time: 246 us
  waiting for transfers between devices  140 us (57%)
  blocking collectives  44.4 us (18%)
  matrix products  20.4 us (8%)
  local copies, waits for them, and re-layouts  14 us (6%)
  between operations  13.6 us (6%)
  other arithmetic  8.01 us (3%)
  starting transfers between devices  5.56 us (2%)
    reduce_scatter x1, waiting for transfers between devices, shards(): lax.psum_scatter(jnp.stack(term_list, axis=2).astype(jnp.bfloat16), 'tp',...  58 us
    all_gather x1, waiting for transfers between devices, shards(): shard_piece = lax.all_gather(received, 'tp', axis=3, tiled=True)  45.5 us
    all_to_all x1, blocking collectives, shards(): lax.all_to_all(send_rows, 'ep', split_axis=0, concat_axis=0, tiled=True)  44.4 us
    all_to_all x1, waiting for transfers between devices, shards(): lax.all_to_all(summed.reshape(quarter, experts * capacity), 'ep', split_a...  36.3 us
    dot_general x1, matrix products, shards(): lax.dot_general(weight_rows, activated[member], (((0,), (1,)), ((), ())),...  11.9 us
    dot_general x1, matrix products, shards(): jnp.dot(row_block, gate_rows, preferred_element_type=jnp.float32)  8.52 us
    all_to_all x1, starting transfers between devices, shards(): lax.all_to_all(summed.reshape(quarter, experts * capacity), 'ep', split_a...  5.51 us
    gather x1, local copies, waits for them, and re-layouts, shards(): source_rows[row_table].reshape(groups, member_count, capacity, quarter)  5.43 us
  transfers between devices with their start and end apart: 3, of which 3 were waited for; matrix products, arithmetic and copies ran while one was open for 0% of the time, Pallas kernels for 0%

commit v1 on v0

--- a/solution.py
+++ b/solution.py
@@ -42,7 +42,7 @@
     send_rows = source_rows[row_table].reshape(groups, member_count, capacity, quarter)
     received = lax.all_to_all(send_rows, "ep", split_axis=0, concat_axis=0, tiled=True)
     slot_count = received.shape[2]
-    shard_piece = lax.all_gather(received, "tp", axis=3, tiled=True)
+    shard_piece = jnp.concatenate(lax.all_gather(received, "tp"), axis=3)
     span_size = shard_piece.shape[3]
     member = 0
     row_block = shard_piece[:, member].reshape(-1, span_size)

time: 246 us -> 261 us (1.061)
  local copies, waits for them, and re-layouts: 14 us -> 32.6 us
  matrix products: 20.4 us -> 17.1 us
    reshape x0 -> x1, local copies, waits for them, and re-layouts: none -> 10.3 us  [shards(): shard_piece = jnp.concatenate(lax.all_gather(received, 'tp'), axis=3)]
    unnamed x8 -> x13, local copies, waits for them, and re-layouts: 1.11 us -> 9.38 us
    dot_general x1, matrix products: 8.52 us -> 5.18 us  [shards(): jnp.dot(row_block, gate_rows, preferred_element_type=jnp.float32)]
where the time goes in v1:
time: 261 us
  waiting for transfers between devices  140 us (54%)
  blocking collectives  44.4 us (17%)
  local copies, waits for them, and re-layouts  32.6 us (12%)
  matrix products  17.1 us (7%)
  between operations  13.6 us (5%)
  other arithmetic  7.98 us (3%)
  starting transfers between devices  5.77 us (2%)
    reduce_scatter x1, waiting for transfers between devices, shards(): lax.psum_scatter(jnp.stack(term_list, axis=2).astype(jnp.bfloat16), 'tp',...  58 us
    all_gather x1, waiting for transfers between devices, shards(): shard_piece = jnp.concatenate(lax.all_gather(received, 'tp'), axis=3)  45.3 us
    all_to_all x1, blocking collectives, shards(): lax.all_to_all(send_rows, 'ep', split_axis=0, concat_axis=0, tiled=True)  44.4 us
    all_to_all x1, waiting for transfers between devices, shards(): lax.all_to_all(summed.reshape(quarter, experts * capacity), 'ep', split_a...  36.3 us
    dot_general x1, matrix products, shards(): lax.dot_general(weight_rows, activated[member], (((0,), (1,)), ((), ())),...  11.9 us
    reshape x1, local copies, waits for them, and re-layouts, shards(): shard_piece = jnp.concatenate(lax.all_gather(received, 'tp'), axis=3)  10.3 us
    unnamed x13, local copies, waits for them, and re-layouts  9.38 us
    all_to_all x1, starting transfers between devices, shards(): lax.all_to_all(summed.reshape(quarter, experts * capacity), 'ep', split_a...  5.54 us
  transfers between devices with their start and end apart: 3, of which 3 were waited for; matrix products, arithmetic and copies ran while one was open for 0% of the time, Pallas kernels for 0%

profile of v1, /device:TPU:0, one launch (start us, length us, event | category | flops | bytes accessed | tf_op | source)
XLA Modules:
  0.0 261.1 jit_solution(1816204147233620051)
XLA Ops:
  6.5 0.0 copy-start
  6.5 0.0 all-gather.3.cloned.1.call-start
  6.5 1.0 copy.25
  7.5 0.1 eq.26
  7.7 0.1 reshape.114
  7.8 0.7 broadcast_multiply_fusion
  8.5 1.1 reduce-window.6
  9.6 0.2 slice_reduce_fusion
  9.9 0.1 fusion.12
  10.0 0.1 copy.29
  10.1 0.1 mul.76
  10.3 2.5 scatter_custom_fusion
  12.8 1.5 fusion.4
  14.3 1.5 fusion.6
  15.9 5.4 %gather_fusion = bf16[1536,512]{1,0:T(8,128)(2,1)} fusion(bf16[257,512]{1,0:T(8,128)(2,1)S(1)} %pad_dynamic-slice_fusion, s32[2048]{0:T(1024)S(1)} %pad_clamp_fusion), kind=kCustom, calls=%fused_computation | custom fusion | bytes 3151872 | tf_op jit(solution)/shard_map/gather | solution.py:42
  21.3 44.4 %all_to_all.17 = bf16[8,1,192,512]{3,2,1,0:T(8,128)(2,1)} all-to-all(bf16[8,1,192,512]{3,2,1,0:T(8,128)(2,1)} %bitcast.47), channel_id=1, replica_groups=mesh['ep'=8,'tp'=4] {'ep'}, dimensions={0} | all-to-all | bytes 3145728 | tf_op jit(solution)/shard_map/all_to_all | solution.py:43
  65.7 0.0 all-gather.3.cloned.1.call-update
  65.8 0.2 reduce-scatter.2.cloned.1.call-start
  66.0 45.3 %all-gather.3.cloned.1.call-done = bf16[32,1,192,512]{3,2,1,0:T(8,128)(2,1)} async-done(((bf16[8,1,192,512]{3,2,1,0:T(8,128)(2,1)}), bf16[32,1,192,512]{3,2,1,0:T(8,128)(2,1)}) %all-gather.3.cloned.1.call-update) | async-done | bytes 6291472 | tf_op jit(solution)/shard_map/all_gather | solution.py:45
  111.3 10.3 %copy.31 = bf16[8,1,192,4,512]{4,3,2,0,1:T(4,128)(2,1)} copy(bf16[8,1,192,4,512]{4,2,0,3,1:T(8,128)(2,1)} %bitcast.43) | data formatting | bytes 12582912 | tf_op jit(solution)/shard_map/reshape | solution.py:45
  121.6 0.0 copy-start.4
  121.6 5.6 %copy.33 = bf16[192,8,4,512]{3,1,2,0:T(8,128)(2,1)S(1)} copy(bf16[192,8,4,512]{3,2,1,0:T(4,128)(2,1)} %bitcast.42) | data formatting | bytes 12582912
  127.2 0.0 copy-start.1
  127.2 2.6 %copy-done.1 = bf16[192,8,4,512]{3,1,2,0:T(8,128)(2,1)} copy-done((bf16[192,8,4,512]{3,1,2,0:T(8,128)(2,1)}, bf16[192,8,4,512]{3,1,2,0:T(8,128)(2,1)S(1)}, u32[]{:S(2)}) %copy-start.1) | copy-done | bytes 6291480
  129.9 0.0 copy-done.4
  129.9 5.2 %convolution_minimum_fusion = f32[1536,512]{1,0:T(8,128)} fusion(bf16[1536,2048]{1,0:T(8,128)(2,1)S(1)} %bitcast.45, bf16[1,2048,512]{2,1,0:T(8,128)(2,1)S(1)} %copy-done.4), kind=kOutput, calls=%fused_computation.5 | convolution fusion | flops 3222011904 | bytes 11534336 | tf_op jit(solution)/shard_map/dot_general | solution.py:51
  135.0 0.0 copy-done
  135.0 11.9 %convolution_convert_fusion = bf16[1536,2048]{1,0:T(8,128)(2,1)} fusion(bf16[1,512,2048]{2,1,0:T(8,128)(2,1)S(1)} %copy-done, f32[1536,512]{1,0:T(8,128)} %convolution_minimum_fusion, bf16[1536,2048]{1,0:T(8,128)(2,1)} %bitcast.46, bf16[1,2048,512]{2,1,0:T(8,128)(2,1)} %param.12), kind=kOutput, calls=%fused_computation.3 | convolution fusion | flops 6452674560 | bytes 19922944 | tf_op jit(solution)/shard_map/dot_general | solution.py:58
  147.0 0.0 reduce-scatter.2.cloned.1.call-update
  147.0 0.0 copy-start.2
  147.0 0.0 copy-start.3
  147.0 58.0 %reduce-scatter.2.cloned.1.call-done = bf16[512,8,1,192]{0,3,1,2:T(8,128)(2,1)} async-done(((bf16[2048,8,1,192]{0,3,1,2:T(8,128)(2,1)}), bf16[512,8,1,192]{0,3,1,2:T(8,128)(2,1)}) %reduce-scatter.2.cloned.1.call-update) | async-done | bytes 1572880 | tf_op jit(solution)/shard_map/reduce_scatter | solution.py:62
  205.0 5.5 %all-to-all-start.1 = ((bf16[512,8,192]{0,2,1:T(8,128)(2,1)}), bf16[512,8,192]{0,2,1:T(8,128)(2,1)}, u32[]{:S(2)}, u32[]{:S(2)}) async-start(bf16[512,8,192]{0,2,1:T(8,128)(2,1)} %bitcast.49), calls=%async_computation.2 | async-start | bytes 3145728 | tf_op jit(solution)/shard_map/all_to_all | solution.py:65
  210.6 0.1 sub.15
  210.7 0.1 copy.27
  210.8 0.0 copy-done.2
  210.8 0.2 copy.28
  211.0 0.0 copy-done.3
  211.0 0.1 copy.32
  211.2 36.3 %all-to-all-done.1 = bf16[512,8,192]{0,2,1:T(8,128)(2,1)} async-done(((bf16[512,8,192]{0,2,1:T(8,128)(2,1)}), bf16[512,8,192]{0,2,1:T(8,128)(2,1)}, u32[]{:S(2)}, u32[]{:S(2)}) %all-to-all-start.1) | async-done | bytes 1572896 | tf_op jit(solution)/shard_map/all_to_all | solution.py:65
  247.5 3.6 %gather_fusion.1 = bf16[512,512]{1,0:T(8,128)(2,1)S(1)} fusion(bf16[512,1536]{0,1:T(8,128)(2,1)} %bitcast.14, s32[1024]{0:T(1024)S(1)} %pad_clamp_fusion.1), kind=kCustom, calls=%fused_computation.1 | custom fusion | bytes 1050624 | tf_op jit(solution)/shard_map/jit(_take)/gather | solution.py:68
  251.1 0.2 gather.11
  251.3 2.9 %multiply_reduce_fusion = bf16[512,256]{0,1:T(8,128)(2,1)} fusion(bf16[512,256,2]{0,2,1:T(2,128)(2,1)S(1)} %gather.11, pred[256,2]{1,0:T(8,128)(4,1)S(1)} %copy.28, f32[256,2]{1,0:T(8,128)S(1)} %copy.32), kind=kLoop, calls=%fused_computation.19 | loop fusion | flops 917504 | bytes 788992 | tf_op jit(solution)/shard_map/reduce_sum | solution.py:69
  (12 shorter events, 0.1 us)
Async XLA Ops:
  6.5 128.5 %copy-start = (bf16[1,512,2048]{2,1,0:T(8,128)(2,1)S(1)}, bf16[1,512,2048]{2,1,0:T(8,128)(2,1)}, u32[]{:S(2)}) copy-start(bf16[1,512,2048]{2,1,0:T(8,128)(2,1)} %param.13) | copy-start | bytes 6291460
  6.5 104.7 %all-gather.3.cloned.1.call-start = ((), (), s32[]{:S(2)}) async-start(), calls=%async_computation.4 | async-start | bytes 7864320 | tf_op jit(solution)/shard_map/all_gather | solution.py:45
  65.8 139.3 %reduce-scatter.2.cloned.1.call-start = ((), (), s32[]{:S(2)}) async-start(), calls=%async_computation.3 | async-start | bytes 7864320 | tf_op jit(solution)/shard_map/reduce_scatter | solution.py:62
  121.6 8.3 %copy-start.4 = (bf16[1,2048,512]{2,1,0:T(8,128)(2,1)S(1)}, bf16[1,2048,512]{2,1,0:T(8,128)(2,1)}, u32[]{:S(2)}) copy-start(bf16[1,2048,512]{2,1,0:T(8,128)(2,1)} %param.11) | copy-start | bytes 6291460
  127.2 2.7 %copy-start.1 = (bf16[192,8,4,512]{3,1,2,0:T(8,128)(2,1)}, bf16[192,8,4,512]{3,1,2,0:T(8,128)(2,1)S(1)}, u32[]{:S(2)}) copy-start(bf16[192,8,4,512]{3,1,2,0:T(8,128)(2,1)S(1)} %copy.33) | copy-start | bytes 18874372
  147.0 63.8 %copy-start.2 = (s32[256,2]{0,1:T(2,128)S(1)}, s32[256,2]{0,1:T(2,128)}, u32[]{:S(2)}) copy-start(s32[256,2]{0,1:T(2,128)} %param.8) | copy-start | bytes 6148
  147.0 64.0 %copy-start.3 = (f32[256,2]{0,1:T(2,128)S(1)}, f32[256,2]{0,1:T(2,128)}, u32[]{:S(2)}) copy-start(f32[256,2]{0,1:T(2,128)} %param.9) | copy-start | bytes 6148
  205.0 42.5 %all-to-all-start.1 = ((bf16[512,8,192]{0,2,1:T(8,128)(2,1)}), bf16[512,8,192]{0,2,1:T(8,128)(2,1)}, u32[]{:S(2)}, u32[]{:S(2)}) async-start(bf16[512,8,192]{0,2,1:T(8,128)(2,1)} %bitcast.49), calls=%async_computation.2 | async-start | bytes 3145728 | tf_op jit(solution)/shard_map/all_to_all | solution.py:65
Sparse Core Ops, SparseCore 0:
  65.9 45.3 all-gather.2
  147.1 57.8 reduce-scatter.1
